TPU v7x, 32 devices: a whole 2x2x4 slice. The times are simulated.
32 devices in a mesh: grp: 2 (over x), kv: 4 (over z), tp: 4 (over y, core).
Axes of the slice: x: 2, y: 2, z: 4, core: 2. Of those that a mesh axis runs over, the one named last changes fastest.
Arguments:
- tokens: bfloat16 [16, 4096], P('grp', 'tp'), parts along dimension 0, may hold values from -50 to 50
- pre_gain: float32 [4096], P('tp'), may hold values from 0.1 to 1.9
- gate_first: bfloat16 [4096, 11264], P('tp', 'kv'), may hold values from -0.09375 to 0.09375
- up_first: bfloat16 [4096, 11264], P('tp', 'kv'), may hold values from -0.09375 to 0.09375
- down_first: bfloat16 [11264, 4096], P('kv', 'tp'), may hold values from -0.0546875 to 0.0546875
- mix_gain: float32 [4096], P('tp'), may hold values from 0.1 to 1.9
- query_w: bfloat16 [4096, 4096], P('tp', 'kv'), may hold values from -0.09375 to 0.09375
- key_w: bfloat16 [4096, 4096], P('tp', 'kv'), may hold values from -0.09375 to 0.09375
- value_w: bfloat16 [4096, 4096], P('tp', 'kv'), may hold values from -0.09375 to 0.09375
- forget_w: bfloat16 [4096, 32], P('tp'), may hold values from -0.09375 to 0.09375
- key_cache: bfloat16 [16, 1024, 4096], P('grp', 'tp', 'kv'), parts along dimension 0, may hold values from -800 to 800
- value_cache: bfloat16 [16, 1024, 4096], P('grp', 'tp', 'kv'), parts along dimension 0, may hold values from -6 to 6
- gate_cache: float32 [16, 32, 1024], P('grp', 'kv', 'tp'), parts along dimension 0, may hold values from -130 to 0, as said below
- lengths: int32 [16], P('grp'), parts along dimension 0, may hold values from 64 to 1024, as said below
- out_w: bfloat16 [4096, 4096], P('kv', 'tp'), may hold values from -0.09375 to 0.09375
- post_gain: float32 [4096], P('tp'), may hold values from 0.1 to 1.9
- gate_second: bfloat16 [4096, 11264], P('tp', 'kv'), may hold values from -0.09375 to 0.09375
- up_second: bfloat16 [4096, 11264], P('tp', 'kv'), may hold values from -0.09375 to 0.09375
- down_second: bfloat16 [11264, 4096], P('kv', 'tp'), may hold values from -0.0546875 to 0.0546875
Outputs:
- out: bfloat16 [16, 4096], P('grp', 'tp'), parts along dimension 0
There are 2 independent parts, one for each index of `grp`. A program takes and returns all parts, laid end to end along the dimension named above; an argument that names none is the same for every part. Nothing has to cross between parts.
Inputs may be any that keep to these rules, and one draw needn't show every extreme that they name: `lengths`: each sequence's count of live cache positions; one sequence has all 1024 in every draw. `gate_cache`: at a live position p of sequence b, the sum of the log forget values of positions p + 1 to lengths[b] - 1 (zero at the last live position); never positive; zero beyond the live positions.
All inputs are finite; a program needn't handle non-finite values.
Results may differ from a plain program's by a relative error of at most 0.015.
Values may be sent and summed in bfloat16 or wider, within the bound.
A program may use at most 128 MiB of HBM per device.

v0:
```python
import jax
import jax.numpy as jnp
from jax import lax
from jax.sharding import PartitionSpec as P

D = 4096
HEAD_DIM = 128
EPSILON = 1e-06
MASKED = -1e30


def half_step(tok_rows, gain_part, w_gate, w_up, w_down):
    widened = tok_rows.astype(jnp.float32)
    squares = jnp.sum(widened * widened, axis=1)
    weighted = (widened * gain_part).astype(jnp.bfloat16)
    gate_part = jnp.dot(weighted, w_gate, preferred_element_type=jnp.float32)
    up_part = jnp.dot(weighted, w_up, preferred_element_type=jnp.float32)
    gate_sum, up_sum, sq_total = (
        lax.psum(gate_part.astype(jnp.bfloat16), "tp").astype(jnp.float32),
        lax.psum(up_part.astype(jnp.bfloat16), "tp").astype(jnp.float32),
        lax.psum(squares.astype(jnp.bfloat16), "tp").astype(jnp.float32),
    )
    norm_scale = lax.rsqrt(sq_total / D + EPSILON)[:, None]
    hidden = (jax.nn.silu(norm_scale * gate_sum) * (norm_scale * up_sum)).astype(jnp.bfloat16)
    down_part = jnp.dot(hidden, w_down, preferred_element_type=jnp.float32)
    down_sum = lax.psum(down_part, "kv")
    return (widened + 0.5 * down_sum).astype(jnp.bfloat16)


def absorb_parts(running, shard_part):
    run_top, run_mass, run_sum = running
    piece_top, masses, piece_sum = shard_part
    new_top = jnp.maximum(run_top, jnp.max(piece_top, axis=0))
    rescale = jnp.exp(run_top - new_top)
    factors = jnp.exp(piece_top - new_top[None])
    run_mass = run_mass * rescale + jnp.sum(masses * factors, axis=0)
    run_sum = run_sum * rescale[:, :, None] + jnp.sum(
        piece_sum.astype(jnp.float32) * factors[:, :, :, None], axis=0
    )
    return (new_top, run_mass, run_sum)


def attention(
    tok_rows,
    mix_gain,
    query_w,
    key_w,
    value_w,
    forget_w,
    key_cache,
    value_cache,
    gate_cache,
    lengths,
):
    widened = tok_rows.astype(jnp.float32)
    squares = jnp.sum(widened * widened, axis=1)
    weighted = (widened * mix_gain).astype(jnp.bfloat16)
    query_part = jnp.dot(weighted, query_w, preferred_element_type=jnp.float32)
    key_part = jnp.dot(weighted, key_w, preferred_element_type=jnp.float32)
    value_part = jnp.dot(weighted, value_w, preferred_element_type=jnp.float32)
    forget_part = jnp.dot(weighted, forget_w, preferred_element_type=jnp.float32)
    query_sum, key_sum, value_sum, forget_sum, sq_total = lax.psum(
        (query_part, key_part, value_part, forget_part, squares), "tp"
    )
    norm_scale = lax.rsqrt(sq_total / D + EPSILON)[:, None]
    query = (norm_scale * query_sum).astype(jnp.bfloat16)
    key_new = (norm_scale * key_sum).astype(jnp.bfloat16)
    value_new = (norm_scale * value_sum).astype(jnp.bfloat16)
    batch_rows = tok_rows.shape[0]
    heads_here = query.shape[1] // HEAD_DIM
    head_start = lax.axis_index("kv") * heads_here
    log_forget = jax.nn.log_sigmoid(
        norm_scale * lax.dynamic_slice_in_dim(forget_sum, head_start, heads_here, 1)
    )
    cache_span = key_cache.shape[1]
    query_heads = query.reshape(batch_rows, heads_here, HEAD_DIM)
    key_block = key_cache.reshape(batch_rows, cache_span, heads_here, HEAD_DIM)
    value_block = value_cache.reshape(batch_rows, cache_span, heads_here, HEAD_DIM)
    scores = jnp.einsum(
        "bhd,bphd->bhp", query_heads, key_block, preferred_element_type=jnp.float32
    ) * HEAD_DIM ** (-0.5)
    scores = scores + gate_cache + log_forget[:, :, None]
    slot_positions = lax.axis_index("tp") * cache_span + lax.iota(jnp.int32, cache_span)
    is_live = slot_positions[None, None, :] < lengths[:, None, None]
    local_top = jnp.max(jnp.where(is_live, scores, MASKED), axis=2)
    local_probs = jnp.where(is_live, jnp.exp(scores - local_top[:, :, None]), 0.0)
    local_mass = jnp.sum(local_probs, axis=2)
    local_sum = jnp.einsum(
        "bhp,bphd->bhd",
        local_probs.astype(jnp.bfloat16),
        value_block,
        preferred_element_type=jnp.float32,
    ).astype(jnp.bfloat16)
    initial = (
        jnp.full((batch_rows, heads_here), MASKED, jnp.float32),
        jnp.zeros((batch_rows, heads_here), jnp.float32),
        jnp.zeros((batch_rows, heads_here, HEAD_DIM), jnp.float32),
    )
    run_top, run_mass, run_sum = absorb_parts(
        initial,
        (
            lax.all_gather(local_top[None].astype(jnp.bfloat16), "tp", axis=0, tiled=True).astype(
                jnp.float32
            ),
            lax.all_gather(local_mass[None].astype(jnp.bfloat16), "tp", axis=0, tiled=True).astype(
                jnp.float32
            ),
            lax.all_gather(local_sum[None], "tp", axis=0, tiled=True),
        ),
    )
    new_heads = key_new.reshape(batch_rows, heads_here, HEAD_DIM).astype(jnp.float32)
    own_score = jnp.sum(query_heads.astype(jnp.float32) * new_heads, axis=2) * HEAD_DIM ** (-0.5)
    highest = jnp.maximum(run_top, own_score)
    rescale = jnp.exp(run_top - highest)
    own_weight = jnp.exp(own_score - highest)
    own_values = value_new.reshape(batch_rows, heads_here, HEAD_DIM).astype(jnp.float32)
    numer = run_sum * rescale[:, :, None] + own_weight[:, :, None] * own_values
    denom = run_mass * rescale + own_weight
    return (
        (numer / denom[:, :, None]).astype(jnp.bfloat16).reshape(batch_rows, heads_here * HEAD_DIM)
    )


def on_device(
    tokens,
    pre_gain,
    gate_first,
    up_first,
    down_first,
    mix_gain,
    query_w,
    key_w,
    value_w,
    forget_w,
    key_cache,
    value_cache,
    gate_cache,
    lengths,
    out_w,
    post_gain,
    gate_second,
    up_second,
    down_second,
):
    after_first = half_step(tokens, pre_gain, gate_first, up_first, down_first)
    attended = attention(
        after_first,
        mix_gain,
        query_w,
        key_w,
        value_w,
        forget_w,
        key_cache,
        value_cache,
        gate_cache,
        lengths,
    )
    projected = lax.psum(jnp.dot(attended, out_w, preferred_element_type=jnp.float32), "kv")
    residual_two = (after_first.astype(jnp.float32) + projected).astype(jnp.bfloat16)
    return half_step(residual_two, post_gain, gate_second, up_second, down_second)


def solution(mesh):
    placed = (
        P("grp", "tp"),
        P("tp"),
        P("tp", "kv"),
        P("tp", "kv"),
        P("kv", "tp"),
        P("tp"),
        P("tp", "kv"),
        P("tp", "kv"),
        P("tp", "kv"),
        P("tp", None),
        P("grp", "tp", "kv"),
        P("grp", "tp", "kv"),
        P("grp", "kv", "tp"),
        P("grp"),
        P("kv", "tp"),
        P("tp"),
        P("tp", "kv"),
        P("tp", "kv"),
        P("kv", "tp"),
    )
    return jax.shard_map(
        on_device, mesh=mesh, in_specs=placed, out_specs=P("grp", "tp"), check_vma=False
    )
```

profile of v0, /device:TPU:0, one launch (start us, length us, event | category | flops | bytes accessed | tf_op | source)
XLA Modules:
  0.0 220.3 jit_solution(18089456365356496139)
XLA Ops:
  6.6 1.5 fusion.15
  8.1 4.5 %convolution_convert_fusion.3 = bf16[8,2816]{1,0:T(8,128)(2,1)} fusion(bf16[1024,2816]{1,0:T(8,128)(2,1)} %param.21, bf16[8,1024]{1,0:T(8,128)(2,1)} %param.19, f32[1024]{0:T(1024)} %param.20), kind=kOutput, calls=%fused_computation.6 | convolution fusion | flops 46184448 | bytes 5832704 | tf_op jit(solution)/shard_map/dot_general | solution.py:16
  12.6 1.5 convolution_convert_fusion.2
  14.1 33.9 %all-reduce.11.cloned.1.call-done = (bf16[8,2816]{1,0:T(8,128)(2,1)}, bf16[8,2816]{1,0:T(8,128)(2,1)}, bf16[8]{0:T(256)(128)(2,1)}) async-done(((bf16[8,2816]{1,0:T(8,128)(2,1)}, bf16[8,2816]{1,0:T(8,128)(2,1)}, bf16[8]{0:T(256)(128)(2,1)}), (bf16[8,2816]{1,0:T(8,128)(2,1)}, bf16[8,2816]{1,0:T(8,128)(2,1)}, bf16[8]{0:T(256)(128)(2,1)})) %all-reduce.11.cloned.1.call-update) | async-done | bytes 90144 | tf_op jit(solution)/shard_map/psum | solution.py:20
  48.1 0.7 add_rsqrt_fusion.2
  48.7 3.6 %fusion.9 = f32[8,1024]{1,0:T(8,128)S(1)} fusion(bf16[2816,1024]{1,0:T(8,128)(2,1)} %param.23, bf16[8,2816]{1,0:T(8,128)(2,1)} %get-tuple-element.13, bf16[8,2816]{1,0:T(8,128)(2,1)} %get-tuple-element.14, f32[8]{0:T(128)S(1)} %add_rsqrt_fusion.2), kind=kOutput, calls=%fused_computation.28 | convolution fusion | flops 46362624 | bytes 5890080 | tf_op jit(solution)/shard_map/dot_general | solution.py:25
  52.3 19.1 %psum.101 = f32[8,1024]{1,0:T(8,128)S(1)} all-reduce(f32[8,1024]{1,0:T(8,128)S(1)} %fusion.9), channel_id=1, replica_groups=mesh['grp'=2,'kv'=4,'tp'=4] {'kv'}, use_global_device_ids=true, to_apply=%region_4.5 | all-reduce | flops 8192 | bytes 65536 | tf_op jit(solution)/shard_map/psum | solution.py:26
  71.4 0.7 fusion.18
  72.2 0.7 fusion.45
  72.9 1.0 fusion.43
  73.9 2.6 %fusion.41 = f32[8,1024]{1,0:T(8,128)} fusion(bf16[1024,1024]{1,0:T(8,128)(2,1)} %param.27, bf16[8,1024]{1,0:T(8,128)(2,1)S(1)} %get-tuple-element.21, f32[1024]{0:T(1024)S(1)} %copy-done.5), kind=kOutput, calls=%fused_computation.68 | convolution fusion | flops 16801792 | bytes 2150400 | tf_op jit(solution)/shard_map/dot_general | solution.py:60
  76.4 1.0 fusion.47
  77.6 6.4 %copy.38 = bf16[8,256,1024]{1,2,0:T(8,128)(2,1)} copy(bf16[8,256,1024]{2,1,0:T(8,128)(2,1)} %param.29) | data formatting | bytes 8388608 | tf_op jit(solution)/shard_map/reshape | solution.py:77
  84.0 21.8 %all-reduce.7.cloned.1.call-done = (f32[8,1024]{1,0:T(8,128)}, f32[8]{0:T(128)}, f32[8,32]{1,0:T(8,128)}, f32[8,1024]{1,0:T(8,128)}, f32[8,1024]{1,0:T(8,128)}) async-done(((f32[8,1024]{1,0:T(8,128)}, f32[8]{0:T(128)}, f32[8,32]{1,0:T(8,128)}, f32[8,1024]{1,0:T(8,128)}, f32[8,1024]{1,0:T(8,128)}), (f32[8,1024]{1,0:T(8,128)}, f32[8]{0:T(128)}, f32[8,32]{1,0:T(8,128)}, f32[8,1024]{1,0:T(8,128)}, ...) | async-done | bytes 99376 | tf_op jit(solution)/shard_map/psum | solution.py:62
  105.8 0.7 add_rsqrt_fusion.1
  106.5 0.8 fusion.54
  107.4 0.9 fusion.27
  108.4 0.8 fusion.51
  109.1 2.8 %fusion.28 = f32[8,8,1,256]{3,2,1,0:T(1,128)S(1)} fusion(bf16[8,256,8,128]{1,3,2,0:T(8,128)(2,1)} %bitcast.68, bf16[8,8,128,1]{2,0,1,3:T(8,128)(2,1)S(1)} %fusion.54), kind=kOutput, calls=%fused_computation.50 | convolution fusion | flops 4194304 | bytes 4276224 | tf_op jit(solution)/shard_map/bhd,bphd->bhp/dot_general | solution.py:79
  112.3 5.2 %all-gather = bf16[32,8]{1,0:T(8,128)(2,1)S(1)} all-gather(bf16[8,8]{1,0:T(8,128)(2,1)S(1)} %convert_element_type.152), channel_id=2, replica_groups=mesh['grp'=2,'kv'=4,'tp'=4] {'tp'}, dimensions={0}, use_global_device_ids=true | all-gather | bytes 640 | tf_op jit(solution)/shard_map/all_gather | solution.py:102
  117.6 5.5 %all-gather.2 = bf16[32,8]{1,0:T(8,128)(2,1)S(1)} all-gather(bf16[8,8]{1,0:T(8,128)(2,1)S(1)} %get-tuple-element.22), channel_id=4, replica_groups=mesh['grp'=2,'kv'=4,'tp'=4] {'tp'}, dimensions={0}, use_global_device_ids=true | all-gather | bytes 640 | tf_op jit(solution)/shard_map/all_gather | solution.py:105
  123.2 3.0 %fusion = f32[8,8,1,128]{3,2,1,0:T(1,128)S(1)} fusion(bf16[8,8,256,1]{2,1,0,3:T(8,128)(2,1)S(1)} %get-tuple-element.23, bf16[8,256,1024]{2,1,0:T(8,128)(2,1)} %param.30), kind=kOutput, calls=%fused_computation | convolution fusion | flops 4194304 | bytes 4259840 | tf_op jit(solution)/shard_map/bhp,bphd->bhd/dot_general | solution.py:88
  126.2 5.2 %all-gather.1 = bf16[32,8,128]{2,1,0:T(8,128)(2,1)S(1)} all-gather(bf16[8,8,128]{2,1,0:T(8,128)(2,1)S(1)} %convert_element_type.155), channel_id=3, replica_groups=mesh['grp'=2,'kv'=4,'tp'=4] {'tp'}, dimensions={0}, use_global_device_ids=true | all-gather | bytes 81920 | tf_op jit(solution)/shard_map/all_gather | solution.py:108
  132.1 19.3 %psum.107 = f32[8,1024]{1,0:T(8,128)S(1)} all-reduce(f32[8,1024]{1,0:T(8,128)S(1)} %fusion.31), channel_id=1, replica_groups=mesh['grp'=2,'kv'=4,'tp'=4] {'kv'}, use_global_device_ids=true, to_apply=%region_17.18 | all-reduce | flops 8192 | bytes 65536 | tf_op jit(solution)/shard_map/psum | solution.py:158
  151.4 0.6 fusion.21
  152.1 4.1 %convolution_convert_fusion.1 = bf16[8,2816]{1,0:T(8,128)(2,1)} fusion(bf16[1024,2816]{1,0:T(8,128)(2,1)} %param.35, bf16[8,1024]{1,0:T(8,128)(2,1)S(1)} %get-tuple-element.17, f32[1024]{0:T(1024)S(1)} %copy-done.10), kind=kOutput, calls=%fused_computation.4 | convolution fusion | flops 46184448 | bytes 5832704 | tf_op jit(solution)/shard_map/dot_general | solution.py:16
  156.2 4.1 %convolution_convert_fusion = bf16[8,2816]{1,0:T(8,128)(2,1)} fusion(bf16[1024,2816]{1,0:T(8,128)(2,1)} %param.36, bf16[8,1024]{1,0:T(8,128)(2,1)S(1)} %get-tuple-element.17, f32[1024]{0:T(1024)S(1)} %copy-done.10), kind=kOutput, calls=%fused_computation.3 | convolution fusion | flops 46184448 | bytes 5832704 | tf_op jit(solution)/shard_map/dot_general | solution.py:17
  160.3 29.6 %all-reduce.9.cloned.1.call-done = (bf16[8,2816]{1,0:T(8,128)(2,1)}, bf16[8,2816]{1,0:T(8,128)(2,1)}, bf16[8]{0:T(256)(128)(2,1)}) async-done(((bf16[8,2816]{1,0:T(8,128)(2,1)}, bf16[8,2816]{1,0:T(8,128)(2,1)}, bf16[8]{0:T(256)(128)(2,1)}), (bf16[8,2816]{1,0:T(8,128)(2,1)}, bf16[8,2816]{1,0:T(8,128)(2,1)}, bf16[8]{0:T(256)(128)(2,1)})) %all-reduce.9.cloned.1.call-update) | async-done | bytes 90144 | tf_op jit(solution)/shard_map/psum | solution.py:20
  190.0 0.7 add_rsqrt_fusion
  190.6 3.6 %fusion.10 = f32[8,1024]{1,0:T(8,128)S(1)} fusion(bf16[2816,1024]{1,0:T(8,128)(2,1)} %param.37, bf16[8,2816]{1,0:T(8,128)(2,1)} %get-tuple-element.10, bf16[8,2816]{1,0:T(8,128)(2,1)} %get-tuple-element.11, f32[8]{0:T(128)S(1)} %add_rsqrt_fusion), kind=kOutput, calls=%fused_computation.29 | convolution fusion | flops 46362624 | bytes 5890080 | tf_op jit(solution)/shard_map/dot_general | solution.py:25
  194.2 19.0 %psum.111 = f32[8,1024]{1,0:T(8,128)S(1)} all-reduce(f32[8,1024]{1,0:T(8,128)S(1)} %fusion.10), channel_id=1, replica_groups=mesh['grp'=2,'kv'=4,'tp'=4] {'kv'}, use_global_device_ids=true, to_apply=%region_22.23 | all-reduce | flops 8192 | bytes 65536 | tf_op jit(solution)/shard_map/psum | solution.py:26
  213.2 0.6 fusion.23
  (46 shorter events, 1.5 us)
Async XLA Ops:
  6.5 66.3 %copy-start = (bf16[1024,1024]{1,0:T(8,128)(2,1)S(1)}, bf16[1024,1024]{1,0:T(8,128)(2,1)}, u32[]{:S(2)}) copy-start(bf16[1024,1024]{1,0:T(8,128)(2,1)} %param.26) | copy-start | bytes 6291460
  6.5 6.0 %copy-start.4 = (bf16[8,1024]{1,0:T(8,128)(2,1)S(1)}, bf16[8,1024]{1,0:T(8,128)(2,1)}, u32[]{:S(2)}) copy-start(bf16[8,1024]{1,0:T(8,128)(2,1)} %param.19) | copy-start | bytes 49156
  6.5 6.0 %copy-start.9 = (f32[1024]{0:T(1024)S(1)}, f32[1024]{0:T(1024)}, u32[]{:S(2)}) copy-start(f32[1024]{0:T(1024)} %param.20) | copy-start | bytes 12292
  6.5 41.5 %all-reduce.11.cloned.1.call-start = ((), (), s32[]{:S(2)}) async-start(), calls=%async_computation.2 | async-start | bytes 181248 | tf_op jit(solution)/shard_map/psum | solution.py:20
  6.5 6.0 %copy-start.1 = (bf16[1024,2816]{1,0:T(8,128)(2,1)S(1)}, bf16[1024,2816]{1,0:T(8,128)(2,1)}, u32[]{:S(2)}) copy-start(bf16[1024,2816]{1,0:T(8,128)(2,1)} %param.22) | copy-start | bytes 17301508
  14.0 58.1 %copy-start.5 = (f32[1024]{0:T(1024)S(1)}, f32[1024]{0:T(1024)}, u32[]{:S(2)}) copy-start(f32[1024]{0:T(1024)} %param.24) | copy-start | bytes 12292
  14.0 58.1 %copy-start.7 = (bf16[1024,32]{0,1:T(8,128)(2,1)S(1)}, bf16[1024,32]{0,1:T(8,128)(2,1)}, u32[]{:S(2)}) copy-start(bf16[1024,32]{0,1:T(8,128)(2,1)} %param.28) | copy-start | bytes 196612
  14.1 91.8 %all-reduce.7.cloned.1.call-start = ((), (), s32[]{:S(2)}) async-start(), calls=%async_computation | async-start | bytes 205824 | tf_op jit(solution)/shard_map/psum | solution.py:62
  52.3 25.2 %copy-start.11 = (s32[8]{0:T(128)S(1)}, s32[8]{0:T(128)}, u32[]{:S(2)}) copy-start(s32[8]{0:T(128)} %param.32) | copy-start | bytes 100
  71.4 5.0 %copy-start.3 = (bf16[1024,1024]{1,0:T(8,128)(2,1)S(1)}, bf16[1024,1024]{1,0:T(8,128)(2,1)}, u32[]{:S(2)}) copy-start(bf16[1024,1024]{1,0:T(8,128)(2,1)} %param.25) | copy-start | bytes 6291460
  77.5 112.5 %all-reduce.9.cloned.1.call-start = ((), (), s32[]{:S(2)}) async-start(), calls=%async_computation.1 | async-start | bytes 181248 | tf_op jit(solution)/shard_map/psum | solution.py:20
  84.0 28.0 %copy-start.6 = (f32[8,8,256]{2,1,0:T(8,128)S(1)}, f32[8,8,256]{2,1,0:T(8,128)}, u32[]{:S(2)}) copy-start(f32[8,8,256]{2,1,0:T(8,128)} %param.31) | copy-start | bytes 196612
  109.1 22.5 %copy-start.8 = (f32[8,1024]{1,0:T(8,128)S(1)}, f32[8,1024]{1,0:T(8,128)}, u32[]{:S(2)}) copy-start(f32[8,1024]{1,0:T(8,128)} %get-tuple-element.9) | copy-start | bytes 98308
  112.0 40.1 %copy-start.10 = (f32[1024]{0:T(1024)S(1)}, f32[1024]{0:T(1024)}, u32[]{:S(2)}) copy-start(f32[1024]{0:T(1024)} %param.34) | copy-start | bytes 12292
  123.2 8.4 %copy-start.2 = (bf16[1024,1024]{1,0:T(8,128)(2,1)S(1)}, bf16[1024,1024]{1,0:T(8,128)(2,1)}, u32[]{:S(2)}) copy-start(bf16[1024,1024]{1,0:T(8,128)(2,1)} %param.33) | copy-start | bytes 6291460
Sparse Core Ops, SparseCore 0:
  14.2 33.8 all-reduce.10
  77.6 28.2 all-reduce.6
  160.4 29.4 all-reduce.8
where the time goes:
time: 221 us; the launch traced here: 220 us
  waiting for transfers between devices  85.4 us (39%)
  blocking collectives  73.4 us (33%)
  matrix products  32.9 us (15%)
  between operations  13.3 us (6%)
  other arithmetic  8.63 us (4%)
  local copies, waits for them, and re-layouts  6.69 us (3%)
    psum x2, waiting for transfers between devices, half_step(): lax.psum(up_part.astype(jnp.bfloat16), 'tp').astype(jnp.float32)  63.5 us
    psum x2, blocking collectives, half_step(): down_sum = lax.psum(down_part, 'kv')  38.1 us
    psum x1, waiting for transfers between devices, attention(): lax.psum((query_part, key_part, value_part, forget_part, squares), 'tp')  21.8 us
    psum x1, blocking collectives, on_device(): lax.psum(jnp.dot(attended, out_w, preferred_element_type=jnp.float32), 'kv')  19.3 us
    dot_general x2, matrix products, half_step(): gate_part = jnp.dot(weighted, w_gate, preferred_element_type=jnp.float32)  8.61 us
    dot_general x2, matrix products, half_step(): down_part = jnp.dot(hidden, w_down, preferred_element_type=jnp.float32)  7.18 us
    reshape x1, local copies, waits for them, and re-layouts, attention(): key_block = key_cache.reshape(batch_rows, cache_span, heads_here, HEAD_DIM)  6.44 us
    dot_general x2, matrix products, half_step(): up_part = jnp.dot(weighted, w_up, preferred_element_type=jnp.float32)  5.58 us
  transfers between devices with their start and end apart: 3, of which 3 were waited for; matrix products, arithmetic and copies ran while one was open for 3% of the time, Pallas kernels for 0%

commit v1 on v0

--- a/solution.py
+++ b/solution.py
@@ -17,7 +17,7 @@
     up_part = jnp.dot(weighted, w_up, preferred_element_type=jnp.float32)
     gate_sum, up_sum, sq_total = (
         lax.psum(gate_part.astype(jnp.bfloat16), "tp").astype(jnp.float32),
-        lax.psum(up_part.astype(jnp.bfloat16), "tp").astype(jnp.float32),
+        jnp.sum(lax.all_gather(up_part.astype(jnp.bfloat16), "tp"), axis=0).astype(jnp.float32),
         lax.psum(squares.astype(jnp.bfloat16), "tp").astype(jnp.float32),
     )
     norm_scale = lax.rsqrt(sq_total / D + EPSILON)[:, None]

time: 221 us -> 184 us (0.83)
  waiting for transfers between devices: 85.4 us -> 21.2 us
  blocking collectives: 73.4 us -> 106 us
  matrix products: 32.9 us -> 30.1 us
  other arithmetic: 8.63 us -> 6.33 us
    psum x2 -> x0, waiting for transfers between devices: 63.5 us -> none  [half_step(): lax.psum(up_part.astype(jnp.bfloat16), 'tp').astype(jnp.float32)]
    psum x0 -> x2, blocking collectives: none -> 23.9 us  [half_step(): lax.psum(gate_part.astype(jnp.bfloat16), 'tp').astype(jnp.float32)]
    all_gather x0 -> x2, blocking collectives: none -> 11.2 us  [half_step(): lax.all_gather(up_part.astype(jnp.bfloat16), 'tp')]
    psum x2, blocking collectives: 38.1 us -> 35.1 us  [half_step(): down_sum = lax.psum(down_part, 'kv')]
    dot_general x2, matrix products: 7.18 us -> 4.44 us  [half_step(): down_part = jnp.dot(hidden, w_down, preferred_element_type=jnp.float32)]
  transfers between devices with their start and end apart: 3 -> 1, of which waited for: 3 -> 1; matrix products, arithmetic and copies ran while one was open for 3% -> 4% of each run, Pallas kernels for 0% -> 0%
where the time goes in v1:
time: 184 us; the launch traced here: 183 us
  blocking collectives  106 us (58%)
  matrix products  30.1 us (16%)
  waiting for transfers between devices  21.2 us (12%)
  between operations  13.6 us (7%)
  local copies, waits for them, and re-layouts  6.7 us (4%)
  other arithmetic  6.33 us (3%)
    psum x2, blocking collectives, half_step(): down_sum = lax.psum(down_part, 'kv')  35.1 us
    psum x2, blocking collectives, half_step(): lax.psum(gate_part.astype(jnp.bfloat16), 'tp').astype(jnp.float32)  23.9 us
    psum x1, waiting for transfers between devices, attention(): lax.psum((query_part, key_part, value_part, forget_part, squares), 'tp')  21.2 us
    psum x1, blocking collectives, on_device(): lax.psum(jnp.dot(attended, out_w, preferred_element_type=jnp.float32), 'kv')  19.3 us
    all_gather x2, blocking collectives, half_step(): lax.all_gather(up_part.astype(jnp.bfloat16), 'tp')  11.2 us
    dot_general x2, matrix products, half_step(): up_part = jnp.dot(weighted, w_up, preferred_element_type=jnp.float32)  7.13 us
    dot_general x2, matrix products, half_step(): gate_part = jnp.dot(weighted, w_gate, preferred_element_type=jnp.float32)  7.01 us
    reshape x1, local copies, waits for them, and re-layouts, attention(): key_block = key_cache.reshape(batch_rows, cache_span, heads_here, HEAD_DIM)  6.44 us
  transfers between devices with their start and end apart: 1, of which 1 were waited for; matrix products, arithmetic and copies ran while one was open for 4% of the time, Pallas kernels for 0%

profile of v1, /device:TPU:0, one launch (start us, length us, event | category | flops | bytes accessed | tf_op | source)
XLA Modules:
  0.0 183.5 jit_solution(16075963529290871718)
XLA Ops:
  6.5 1.0 fusion.15
  7.5 3.5 %convolution_convert_fusion.3 = bf16[8,2816]{1,0:T(8,128)(2,1)S(1)} fusion(bf16[1024,2816]{1,0:T(8,128)(2,1)} %param.21, bf16[8,1024]{1,0:T(8,128)(2,1)} %param.19, f32[1024]{0:T(1024)} %param.20), kind=kOutput, calls=%fused_computation.6 | convolution fusion | flops 46184448 | bytes 5832704 | tf_op jit(solution)/shard_map/dot_general | solution.py:16
  11.1 13.3 %all-reduce.2 = (bf16[8,2816]{1,0:T(8,128)(2,1)S(1)}, bf16[8]{0:T(256)(128)(2,1)S(1)}) all-reduce(bf16[8,2816]{1,0:T(8,128)(2,1)S(1)} %convolution_convert_fusion.3, bf16[8]{0:T(256)(128)(2,1)S(1)} %fusion.15), channel_id=1, replica_groups=mesh['grp'=2,'kv'=4,'tp'=4] {'tp'}, use_global_device_ids=true, to_apply=%region_2.0 | all-reduce | flops 22536 | bytes 90144 | tf_op jit(solution)/shard_map/psum | solution.py:19
  24.4 3.6 %convolution_convert_fusion.2 = bf16[8,2816]{1,0:T(8,128)(2,1)S(1)} fusion(bf16[1024,2816]{1,0:T(8,128)(2,1)} %param.22, bf16[8,1024]{1,0:T(8,128)(2,1)S(1)} %copy-done.4, f32[1024]{0:T(1024)S(1)} %copy-done.9), kind=kOutput, calls=%fused_computation.5 | convolution fusion | flops 46184448 | bytes 5832704 | tf_op jit(solution)/shard_map/dot_general | solution.py:17
  28.1 5.7 %all-gather = bf16[32,2816]{1,0:T(8,128)(2,1)S(1)} all-gather(bf16[8,2816]{1,0:T(8,128)(2,1)S(1)} %convolution_convert_fusion.2), channel_id=2, replica_groups=mesh['grp'=2,'kv'=4,'tp'=4] {'tp'}, dimensions={0}, use_global_device_ids=true | all-gather | bytes 225280 | tf_op jit(solution)/shard_map/all_gather | solution.py:20
  33.8 0.9 fusion.9
  34.7 19.4 %psum.86 = f32[8,1024]{1,0:T(8,128)S(1)} all-reduce(f32[8,1024]{1,0:T(8,128)S(1)} %fusion.9), channel_id=1, replica_groups=mesh['grp'=2,'kv'=4,'tp'=4] {'kv'}, use_global_device_ids=true, to_apply=%region_4.5 | all-reduce | flops 8192 | bytes 65536 | tf_op jit(solution)/shard_map/psum | solution.py:26
  54.1 0.7 fusion.18
  54.8 0.7 fusion.45
  55.5 1.0 fusion.43
  56.5 2.6 %fusion.41 = f32[8,1024]{1,0:T(8,128)} fusion(bf16[1024,1024]{1,0:T(8,128)(2,1)} %param.27, bf16[8,1024]{1,0:T(8,128)(2,1)S(1)} %get-tuple-element.19, f32[1024]{0:T(1024)S(1)} %copy-done.5), kind=kOutput, calls=%fused_computation.70 | convolution fusion | flops 16801792 | bytes 2150400 | tf_op jit(solution)/shard_map/dot_general | solution.py:60
  59.1 1.0 fusion.47
  60.2 6.4 %copy.38 = bf16[8,256,1024]{1,2,0:T(8,128)(2,1)} copy(bf16[8,256,1024]{2,1,0:T(8,128)(2,1)} %param.29) | data formatting | bytes 8388608 | tf_op jit(solution)/shard_map/reshape | solution.py:77
  66.6 21.2 %all-reduce.5.cloned.1.call-done = (f32[8,1024]{1,0:T(8,128)}, f32[8]{0:T(128)}, f32[8,32]{1,0:T(8,128)}, f32[8,1024]{1,0:T(8,128)}, f32[8,1024]{1,0:T(8,128)}) async-done(((f32[8,1024]{1,0:T(8,128)}, f32[8]{0:T(128)}, f32[8,32]{1,0:T(8,128)}, f32[8,1024]{1,0:T(8,128)}, f32[8,1024]{1,0:T(8,128)}), (f32[8,1024]{1,0:T(8,128)}, f32[8]{0:T(128)}, f32[8,32]{1,0:T(8,128)}, f32[8,1024]{1,0:T(8,128)}, ...) | async-done | bytes 99376 | tf_op jit(solution)/shard_map/psum | solution.py:62
  87.8 0.7 add_rsqrt_fusion.1
  88.5 0.8 fusion.54
  89.3 0.9 fusion.27
  90.3 0.8 fusion.51
  91.1 2.8 %fusion.28 = f32[8,8,1,256]{3,2,1,0:T(1,128)S(1)} fusion(bf16[8,256,8,128]{1,3,2,0:T(8,128)(2,1)} %bitcast.72, bf16[8,8,128,1]{2,0,1,3:T(8,128)(2,1)S(1)} %fusion.54), kind=kOutput, calls=%fused_computation.52 | convolution fusion | flops 4194304 | bytes 4276224 | tf_op jit(solution)/shard_map/bhd,bphd->bhp/dot_general | solution.py:79
  94.3 5.2 %all-gather.1 = bf16[32,8]{1,0:T(8,128)(2,1)S(1)} all-gather(bf16[8,8]{1,0:T(8,128)(2,1)S(1)} %convert_element_type.156), channel_id=3, replica_groups=mesh['grp'=2,'kv'=4,'tp'=4] {'tp'}, dimensions={0}, use_global_device_ids=true | all-gather | bytes 640 | tf_op jit(solution)/shard_map/all_gather | solution.py:102
  99.5 5.5 %all-gather.3 = bf16[32,8]{1,0:T(8,128)(2,1)S(1)} all-gather(bf16[8,8]{1,0:T(8,128)(2,1)S(1)} %get-tuple-element.20), channel_id=5, replica_groups=mesh['grp'=2,'kv'=4,'tp'=4] {'tp'}, dimensions={0}, use_global_device_ids=true | all-gather | bytes 640 | tf_op jit(solution)/shard_map/all_gather | solution.py:105
  105.2 3.0 %fusion = f32[8,8,1,128]{3,2,1,0:T(1,128)S(1)} fusion(bf16[8,8,256,1]{2,1,0,3:T(8,128)(2,1)S(1)} %get-tuple-element.21, bf16[8,256,1024]{2,1,0:T(8,128)(2,1)} %param.30), kind=kOutput, calls=%fused_computation | convolution fusion | flops 4194304 | bytes 4259840 | tf_op jit(solution)/shard_map/bhp,bphd->bhd/dot_general | solution.py:88
  108.2 5.2 %all-gather.2 = bf16[32,8,128]{2,1,0:T(8,128)(2,1)S(1)} all-gather(bf16[8,8,128]{2,1,0:T(8,128)(2,1)S(1)} %convert_element_type.159), channel_id=4, replica_groups=mesh['grp'=2,'kv'=4,'tp'=4] {'tp'}, dimensions={0}, use_global_device_ids=true | all-gather | bytes 81920 | tf_op jit(solution)/shard_map/all_gather | solution.py:108
  113.6 0.4 fusion.31
  114.1 19.3 %psum.92 = f32[8,1024]{1,0:T(8,128)S(1)} all-reduce(f32[8,1024]{1,0:T(8,128)S(1)} %fusion.31), channel_id=1, replica_groups=mesh['grp'=2,'kv'=4,'tp'=4] {'kv'}, use_global_device_ids=true, to_apply=%region_17.18 | all-reduce | flops 8192 | bytes 65536 | tf_op jit(solution)/shard_map/psum | solution.py:158
  133.6 3.5 %convolution_convert_fusion.1 = bf16[8,2816]{1,0:T(8,128)(2,1)S(1)} fusion(bf16[1024,2816]{1,0:T(8,128)(2,1)} %param.35, bf16[8,1024]{1,0:T(8,128)(2,1)S(1)} %get-tuple-element.15, f32[1024]{0:T(1024)S(1)} %copy-done.10), kind=kOutput, calls=%fused_computation.4 | convolution fusion | flops 46184448 | bytes 5832704 | tf_op jit(solution)/shard_map/dot_general | solution.py:16
  137.0 10.6 %all-reduce.1 = (bf16[8,2816]{1,0:T(8,128)(2,1)S(1)}, bf16[8]{0:T(256)(128)(2,1)S(1)}) all-reduce(bf16[8,2816]{1,0:T(8,128)(2,1)S(1)} %convolution_convert_fusion.1, bf16[8]{0:T(256)(128)(2,1)S(1)} %get-tuple-element.14), channel_id=1, replica_groups=mesh['grp'=2,'kv'=4,'tp'=4] {'tp'}, use_global_device_ids=true, to_apply=%region_20.21 | all-reduce | flops 22536 | bytes 90144 | tf_op jit(solution)/shard_map/psum | solution.py:19
  147.6 3.5 %convolution_convert_fusion = bf16[8,2816]{1,0:T(8,128)(2,1)S(1)} fusion(bf16[1024,2816]{1,0:T(8,128)(2,1)} %param.36, bf16[8,1024]{1,0:T(8,128)(2,1)S(1)} %get-tuple-element.15, f32[1024]{0:T(1024)S(1)} %copy-done.10), kind=kOutput, calls=%fused_computation.3 | convolution fusion | flops 46184448 | bytes 5832704 | tf_op jit(solution)/shard_map/dot_general | solution.py:17
  151.1 5.5 %all-gather.4 = bf16[32,2816]{1,0:T(8,128)(2,1)S(1)} all-gather(bf16[8,2816]{1,0:T(8,128)(2,1)S(1)} %convolution_convert_fusion), channel_id=6, replica_groups=mesh['grp'=2,'kv'=4,'tp'=4] {'tp'}, dimensions={0}, use_global_device_ids=true | all-gather | bytes 225280 | tf_op jit(solution)/shard_map/all_gather | solution.py:20
  156.7 3.5 %fusion.10 = f32[8,1024]{1,0:T(8,128)S(1)} fusion(bf16[2816,1024]{1,0:T(8,128)(2,1)} %param.37, bf16[8,2816]{1,0:T(8,128)(2,1)S(1)} %bitcast_reduce_fusion, bf16[8,2816]{1,0:T(8,128)(2,1)S(1)} %get-tuple-element.10, f32[8]{0:T(128)S(1)} %add_rsqrt_fusion), kind=kOutput, calls=%fused_computation.31 | convolution fusion | flops 46362624 | bytes 5890080 | tf_op jit(solution)/shard_map/dot_general | solution.py:25
  160.2 15.8 %psum.95 = f32[8,1024]{1,0:T(8,128)S(1)} all-reduce(f32[8,1024]{1,0:T(8,128)S(1)} %fusion.10), channel_id=1, replica_groups=mesh['grp'=2,'kv'=4,'tp'=4] {'kv'}, use_global_device_ids=true, to_apply=%region_22.23 | all-reduce | flops 8192 | bytes 65536 | tf_op jit(solution)/shard_map/psum | solution.py:26
  176.0 0.6 fusion.23
  (46 shorter events, 1.1 us)
Async XLA Ops:
  6.5 49.0 %copy-start = (bf16[1024,1024]{1,0:T(8,128)(2,1)S(1)}, bf16[1024,1024]{1,0:T(8,128)(2,1)}, u32[]{:S(2)}) copy-start(bf16[1024,1024]{1,0:T(8,128)(2,1)} %param.26) | copy-start | bytes 6291460
  6.5 17.9 %copy-start.4 = (bf16[8,1024]{1,0:T(8,128)(2,1)S(1)}, bf16[8,1024]{1,0:T(8,128)(2,1)}, u32[]{:S(2)}) copy-start(bf16[8,1024]{1,0:T(8,128)(2,1)} %param.19) | copy-start | bytes 49156
  6.5 17.9 %copy-start.9 = (f32[1024]{0:T(1024)S(1)}, f32[1024]{0:T(1024)}, u32[]{:S(2)}) copy-start(f32[1024]{0:T(1024)} %param.20) | copy-start | bytes 12292
  6.5 81.3 %all-reduce.5.cloned.1.call-start = ((), (), s32[]{:S(2)}) async-start(), calls=%async_computation | async-start | bytes 205824 | tf_op jit(solution)/shard_map/psum | solution.py:62
  24.4 9.4 %copy-start.1 = (bf16[2816,1024]{1,0:T(8,128)(2,1)S(1)}, bf16[2816,1024]{1,0:T(8,128)(2,1)}, u32[]{:S(2)}) copy-start(bf16[2816,1024]{1,0:T(8,128)(2,1)} %param.23) | copy-start | bytes 17301508
  28.1 26.7 %copy-start.5 = (f32[1024]{0:T(1024)S(1)}, f32[1024]{0:T(1024)}, u32[]{:S(2)}) copy-start(f32[1024]{0:T(1024)} %param.24) | copy-start | bytes 12292
  28.1 26.7 %copy-start.7 = (bf16[1024,32]{0,1:T(8,128)(2,1)S(1)}, bf16[1024,32]{0,1:T(8,128)(2,1)}, u32[]{:S(2)}) copy-start(bf16[1024,32]{0,1:T(8,128)(2,1)} %param.28) | copy-start | bytes 196612
  34.7 25.4 %copy-start.11 = (s32[8]{0:T(128)S(1)}, s32[8]{0:T(128)}, u32[]{:S(2)}) copy-start(s32[8]{0:T(128)} %param.32) | copy-start | bytes 100
  54.1 5.0 %copy-start.3 = (bf16[1024,1024]{1,0:T(8,128)(2,1)S(1)}, bf16[1024,1024]{1,0:T(8,128)(2,1)}, u32[]{:S(2)}) copy-start(bf16[1024,1024]{1,0:T(8,128)(2,1)} %param.25) | copy-start | bytes 6291460
  66.6 27.3 %copy-start.6 = (f32[8,8,256]{2,1,0:T(8,128)S(1)}, f32[8,8,256]{2,1,0:T(8,128)}, u32[]{:S(2)}) copy-start(f32[8,8,256]{2,1,0:T(8,128)} %param.31) | copy-start | bytes 196612
  91.1 22.5 %copy-start.8 = (f32[8,1024]{1,0:T(8,128)S(1)}, f32[8,1024]{1,0:T(8,128)}, u32[]{:S(2)}) copy-start(f32[8,1024]{1,0:T(8,128)} %get-tuple-element.9) | copy-start | bytes 98308
  94.0 39.6 %copy-start.10 = (f32[1024]{0:T(1024)S(1)}, f32[1024]{0:T(1024)}, u32[]{:S(2)}) copy-start(f32[1024]{0:T(1024)} %param.34) | copy-start | bytes 12292
  105.2 8.4 %copy-start.2 = (bf16[1024,1024]{1,0:T(8,128)(2,1)S(1)}, bf16[1024,1024]{1,0:T(8,128)(2,1)}, u32[]{:S(2)}) copy-start(bf16[1024,1024]{1,0:T(8,128)(2,1)} %param.33) | copy-start | bytes 6291460
Sparse Core Ops, SparseCore 0:
  60.2 27.5 all-reduce.4
